TPU v7x, 512 devices: a 8x2x16 block of a 8x16x16 slice. The times are simulated.
512 devices in a mesh: grp: 2 (over y), fs: 16 (over z), tp: 16 (over x, core).
Axes of the slice: x: 8, y: 2, z: 16, core: 2. Of those that a mesh axis runs over, the one named last changes fastest.
The devices are a block of a 8x16x16 slice.
Arguments:
- tokens: bfloat16 [4096, 2048], P(('grp', 'fs'), 'tp'), parts along dimension 0, may hold values from -40 to 40
- norm_gain: float32 [2048], P('tp'), may hold values from 0.1 to 1.9
- expert_ids: int32 [4096, 8], P(('grp', 'fs')), parts along dimension 0, may hold values from 0 to 63, all different within a row; in each aligned block of 128 rows (0 to 127, 128 to 255, ...) at most 24 rows name the same one
- route_scores: float32 [4096, 8], P(('grp', 'fs')), parts along dimension 0, may hold values from 0.1 to 1
- gate_weight: float32 [64, 512, 2048], P(None, 'fs', 'tp'), may hold values from -0.125 to 0.125
- up_weight: float32 [64, 512, 2048], P(None, 'fs', 'tp'), may hold values from -0.125 to 0.125
- down_weight: float32 [64, 512, 2048], P(None, 'fs', 'tp'), may hold values from -0.25 to 0.25
- shared_gate: float32 [512, 2048], P('fs', 'tp'), may hold values from -0.125 to 0.125
- shared_up: float32 [512, 2048], P('fs', 'tp'), may hold values from -0.125 to 0.125
- shared_down: float32 [512, 2048], P('fs', 'tp'), may hold values from -0.25 to 0.25
Outputs:
- gate_served: bfloat16 [128, 512, 2048], P(('grp', 'fs'), None, 'tp'), parts along dimension 0
- up_served: bfloat16 [128, 512, 2048], P(('grp', 'fs'), None, 'tp'), parts along dimension 0
- down_served: bfloat16 [128, 512, 2048], P(('grp', 'fs'), None, 'tp'), parts along dimension 0
- shared_gate_served: bfloat16 [1024, 2048], P('grp', 'tp'), parts along dimension 0
- shared_up_served: bfloat16 [1024, 2048], P('grp', 'tp'), parts along dimension 0
- shared_down_served: bfloat16 [1024, 2048], P('grp', 'tp'), parts along dimension 0
- layer_output: bfloat16 [4096, 2048], P(('grp', 'fs'), 'tp'), parts along dimension 0
There are 2 independent parts, one for each index of `grp`. A program takes and returns all parts, laid end to end along the dimension named above; an argument that names none is the same for every part. Nothing has to cross between parts.
Inputs may be any that keep to these rules, and one draw needn't show every extreme that they name: `expert_ids`: each row names 8 different experts. Among the rows of one index of fs no expert is named more than 24 times; in every draw some expert reaches 24 on some index of fs.
All inputs are finite; a program needn't handle non-finite values.
Results may differ from a plain program's by a relative error of at most 0.03.
Values may be sent and summed in bfloat16 or wider, within the bound.
A program may use at most 64 MiB of HBM per device.

v0:
```python
import jax
import jax.numpy as jnp
from jax import lax
from jax.sharding import Mesh
from jax.sharding import PartitionSpec as P

CAPACITY = 24
TP = ("tp_0", "tp_1")


norm_eps = 1e-05
routed_scale = 2.5


def copy_for_each(array, axis):
    size = lax.axis_size(axis)
    return lax.all_to_all(
        jnp.broadcast_to(array[None], (size, *array.shape)), axis, 0, 0, tiled=True
    )


def of_everyone(array, axis):
    return copy_for_each(array, axis).sum(axis=0)


def in_one(arrays, axis):
    ends = [0]
    for a in arrays:
        ends.append(ends[-1] + a.size)
    total = of_everyone(jnp.concatenate([a.ravel() for a in arrays]), axis)
    return tuple((total[b:e].reshape(a.shape) for a, b, e in zip(arrays, ends, ends[1:])))


def in_one_piece(arrays, axis, dim, along):
    both = jnp.concatenate(arrays, axis=along)
    result, at, finished = (lax.all_gather(both, axis, axis=dim, tiled=True), 0, [])
    for a in arrays:
        finished.append(lax.slice_in_dim(result, at, at + a.shape[along], axis=along))
        at += a.shape[along]
    return tuple(finished)


def side_by_side(arrays, axis, split_dim, concat_dim, along):
    both = jnp.concatenate(arrays, axis=along)
    result, at, finished = (
        lax.all_to_all(both, axis, split_axis=split_dim, concat_axis=concat_dim, tiled=True),
        0,
        [],
    )
    for a in arrays:
        finished.append(lax.slice_in_dim(result, at, at + a.shape[along], axis=along))
        at += a.shape[along]
    return tuple(finished)


def whole_of(array, axes, dim):
    for axis in reversed(axes):
        array = lax.all_gather(array, axis, axis=dim, tiled=True)
    return array


def on_device(
    tokens,
    norm_gain,
    expert_ids,
    route_scores,
    gate_weight,
    up_weight,
    down_weight,
    shared_gate,
    shared_up,
    shared_down,
):
    tok_float = tokens.astype(jnp.float32)
    row_sum, row_squares = in_one(
        (jnp.sum(tok_float, axis=1), jnp.sum(tok_float * tok_float, axis=1)), TP
    )
    full_width = tok_float.shape[1] * lax.axis_size(TP)
    row_mean = row_sum / full_width
    row_var = row_squares / full_width - row_mean * row_mean
    normed = ((tok_float - row_mean[:, None]) * lax.rsqrt(row_var + norm_eps)[:, None]).astype(
        jnp.bfloat16
    )
    gate_new = (gate_weight * norm_gain[None, None, :]).astype(jnp.bfloat16)
    up_new = (up_weight * norm_gain[None, None, :]).astype(jnp.bfloat16)
    down_new = down_weight.astype(jnp.bfloat16)
    gate_shared = (shared_gate * norm_gain[None, :]).astype(jnp.bfloat16)
    up_shared = (shared_up * norm_gain[None, :]).astype(jnp.bfloat16)
    down_shared = shared_down.astype(jnp.bfloat16)
    gate_whole, up_whole, down_whole = in_one_piece(
        (gate_shared, up_shared, down_shared), "fs", 0, 1
    )
    gate_local, up_local = side_by_side((gate_new, up_new), "fs", 0, 1, 2)
    shard_count = lax.axis_size("fs")
    experts_all = gate_weight.shape[0]
    experts_here = experts_all // shard_count
    tok_rows, top_count = expert_ids.shape
    slice_width = normed.shape[1]
    flat_ids = expert_ids.reshape(-1)
    one_hot = (flat_ids[:, None] == jnp.arange(experts_all, dtype=jnp.int32)[None, :]).astype(
        jnp.int32
    )
    earlier = jnp.sum((jnp.cumsum(one_hot, axis=0) - one_hot) * one_hot, axis=1)
    position = (
        flat_ids % experts_here * shard_count + flat_ids // experts_here
    ) * CAPACITY + earlier
    routed_rows = experts_all * CAPACITY
    source_row = (
        jnp.full((routed_rows,), tok_rows, jnp.int32)
        .at[position]
        .set(jnp.arange(flat_ids.shape[0], dtype=jnp.int32) // top_count)
    )
    padded = jnp.concatenate([normed, jnp.zeros((1, slice_width), jnp.bfloat16)], axis=0)
    outgoing = padded[source_row].reshape(experts_here, shard_count, CAPACITY, slice_width)
    arrived = lax.all_to_all(outgoing, "fs", split_axis=1, concat_axis=1, tiled=True)
    rows_in = arrived.reshape(experts_here, shard_count * CAPACITY, slice_width)
    paired = jnp.concatenate([gate_local, up_local], axis=1)
    hidden_width = paired.shape[1] // 2
    routed_terms = jnp.einsum("erd,efd->erf", rows_in, paired, preferred_element_type=jnp.float32)
    shared_pair = jnp.concatenate([gate_whole, up_whole], axis=0)
    shared_terms = lax.dot_general(
        normed, shared_pair, (((1,), (1,)), ((), ())), preferred_element_type=jnp.float32
    )
    all_terms = jnp.concatenate(
        [routed_terms.reshape(routed_rows, 2 * hidden_width), shared_terms], axis=0
    )
    down_local = lax.all_to_all(down_new, "fs", split_axis=0, concat_axis=1, tiled=True)
    row_share = lax.psum_scatter(
        all_terms.astype(jnp.bfloat16), TP, scatter_dimension=0, tiled=True
    ).astype(jnp.float32)
    hidden_part = (jax.nn.silu(row_share[:, :hidden_width]) * row_share[:, hidden_width:]).astype(
        jnp.bfloat16
    )
    hidden = whole_of(hidden_part, TP, 0)
    expert_hidden = hidden[:routed_rows].reshape(experts_here, shard_count * CAPACITY, hidden_width)
    outputs = jnp.einsum(
        "erf,efd->erd", expert_hidden, down_local, preferred_element_type=jnp.float32
    ).astype(jnp.bfloat16)
    returned = lax.all_to_all(
        outputs.reshape(experts_here, shard_count, CAPACITY, slice_width),
        "fs",
        split_axis=1,
        concat_axis=1,
        tiled=True,
    )
    returned = returned.reshape(routed_rows, slice_width)
    route_weight = route_scores / jnp.sum(route_scores, axis=1, keepdims=True) * routed_scale
    picked = returned[position].astype(jnp.float32) * route_weight.reshape(-1)[:, None]
    routed = jnp.sum(picked.reshape(tok_rows, top_count, slice_width), axis=1)
    shared_out = jnp.dot(hidden[routed_rows:], down_whole, preferred_element_type=jnp.float32)
    layer_out = (shared_out + routed).astype(jnp.bfloat16)
    return (gate_local, up_local, down_local, gate_whole, up_whole, down_whole, layer_out)


def solution(mesh):
    split = Mesh(
        mesh.devices.reshape(mesh.shape["grp"], mesh.shape["fs"], 8, 2),
        ("grp", "fs", "tp_0", "tp_1"),
    )
    return jax.shard_map(
        on_device,
        mesh=split,
        in_specs=(
            P(("grp", "fs"), TP),
            P(TP),
            P(("grp", "fs"), None),
            P(("grp", "fs"), None),
            P(None, "fs", TP),
            P(None, "fs", TP),
            P(None, "fs", TP),
            P("fs", TP),
            P("fs", TP),
            P("fs", TP),
        ),
        out_specs=(
            P(("grp", "fs"), None, TP),
            P(("grp", "fs"), None, TP),
            P(("grp", "fs"), None, TP),
            P("grp", TP),
            P("grp", TP),
            P("grp", TP),
            P(("grp", "fs"), TP),
        ),
        check_vma=False,
    )
```

profile of v0, /device:TPU:66, one launch (start us, length us, event | category | flops | bytes accessed | tf_op | source)
XLA Modules:
  0.0 358.9 jit_solution(13174853483276449634)
XLA Ops:
  7.2 0.9 convert_reduce_fusion
  8.1 0.6 broadcast_in_dim.6
  8.8 43.7 %all-to-all-start.2 = ((f32[16,1,256]{2,1,0:T(1,128)}), f32[16,1,256]{2,1,0:T(1,128)S(1)}, u32[]{:S(2)}, u32[]{:S(2)}) async-start(f32[16,1,256]{2,1,0:T(1,128)} %broadcast_in_dim.6), calls=%async_computation.2 | async-start | bytes 32768 | tf_op jit(solution)/shard_map/all_to_all | solution.py:17
  52.5 0.8 copy.55
  53.3 0.1 eq.31
  53.4 0.1 eq.27
  53.4 0.1 reshape.194
  53.6 18.0 %reduce-window.6 = s32[64,8,128]{2,1,0:T(8,128)S(1)} reduce-window(s32[64,8,128]{2,1,0:T(8,128)S(1)} %fusion.11, s32[]{:T(128)} %constant.59.clone.1), window={size=1x1x128 pad=0_0x0_0x127_0}, to_apply=%region_3.0 | reduce-window | flops 8323072 | bytes 524292 | tf_op jit(solution)/shard_map/reduce-window
  71.6 0.1 slice.61
  71.7 0.1 copy.58
  71.9 0.1 copy.59
  72.0 0.1 broadcast_add_fusion
  72.1 0.1 fusion.7
  72.3 4.3 %scatter_custom_fusion = s32[1536]{0:T(1024)S(1)} fusion(s32[1024]{0:T(1024)S(1)} %bitcast.56, s32[1024]{0:T(1024)S(1)} %add_select_fusion, s32[]{:T(128)} %constant.58.clone.1), kind=kCustom, calls=%fused_computation.57 | custom fusion | bytes 6148 | tf_op jit(solution)/shard_map/scatter | solution.py:111
  76.7 0.1 fusion.16
  76.8 0.6 copy-done.10
  77.4 3.2 gather_fusion
  80.6 0.8 copy.60
  81.4 7.7 %all-to-all-start.3 = ((bf16[4,16,24,128]{3,2,0,1:T(8,128)(2,1)}), bf16[4,16,24,128]{3,2,0,1:T(8,128)(2,1)S(1)}, u32[]{:S(2)}, u32[]{:S(2)}) async-start(bf16[4,16,24,128]{3,2,0,1:T(8,128)(2,1)} %copy.60), calls=%async_computation.3 | async-start | bytes 786432 | tf_op jit(solution)/shard_map/all_to_all | solution.py:115
  89.2 0.2 multiply_convert_fusion.1
  89.4 1.1 pad_maximum_fusion.1
  90.6 22.6 %all-to-all-done.3 = bf16[4,16,24,128]{3,2,0,1:T(8,128)(2,1)S(1)} async-done(((bf16[4,16,24,128]{3,2,0,1:T(8,128)(2,1)}), bf16[4,16,24,128]{3,2,0,1:T(8,128)(2,1)S(1)}, u32[]{:S(2)}, u32[]{:S(2)}) %all-to-all-start.3) | async-done | bytes 393248 | tf_op jit(solution)/shard_map/all_to_all | solution.py:115
  113.2 6.0 %all-to-all-start = ((bf16[64,32,256]{2,1,0:T(8,128)(2,1)}), bf16[64,32,256]{2,1,0:T(8,128)(2,1)S(1)}, u32[]{:S(2)}, u32[]{:S(2)}) async-start(bf16[64,32,256]{2,1,0:T(8,128)(2,1)} %pad_maximum_fusion.1), calls=%async_computation | async-start | bytes 2097152 | tf_op jit(solution)/shard_map/all_to_all | solution.py:46
  119.2 0.1 reduce-scatter.2.cloned.1.call-start
  119.3 73.0 %all_gather.9 = bf16[512,384]{1,0:T(8,128)(2,1)S(1)} all-gather(bf16[32,384]{1,0:T(8,128)(2,1)S(1)} %pad_maximum_fusion.2), channel_id=1, replica_groups=mesh['grp'=2,'fs'=16,'tp_0'=8,'tp_1'=2] {'fs'}, dimensions={0}, use_global_device_ids=true | all-gather | bytes 417792 | tf_op jit(solution)/shard_map/all_gather | solution.py:36
  192.4 0.1 fusion.27
  192.5 0.2 convolution_convert_fusion.2
  192.8 0.1 copy.52
  192.9 0.2 fusion.26
  193.1 1.0 convolution_convert_fusion
  194.1 2.0 pad_maximum_fusion
  196.3 0.1 all-gather.2.cloned.1.call-start
  196.3 65.2 %reduce-scatter.2.cloned.1.call-done = bf16[104,1024]{1,0:T(8,128)(2,1)} async-done(((bf16[1664,1024]{1,0:T(8,128)(2,1)}), bf16[104,1024]{1,0:T(8,128)(2,1)}) %reduce-scatter.2.cloned.1.call-update) | async-done | bytes 213008 | tf_op jit(solution)/shard_map/reduce_scatter | solution.py:128
  261.5 1.0 convert_element_type.61
  262.5 0.1 fusion.12
  262.6 2.1 all_gather.10
  264.8 0.1 convert_element_type.53
  264.9 41.8 %all_to_all.52 = bf16[64,32,128]{2,1,0:T(8,128)(2,1)S(1)} all-to-all(bf16[64,32,128]{2,1,0:T(8,128)(2,1)S(1)} %convert_element_type.53), channel_id=1, replica_groups=mesh['grp'=2,'fs'=16,'tp_0'=8,'tp_1'=2] {'fs'}, dimensions={0} | all-to-all | bytes 1048576 | tf_op jit(solution)/shard_map/all_to_all | solution.py:127
  306.7 6.7 %all-gather.2.cloned.1.call-done = bf16[1664,512]{1,0:T(8,128)(2,1)} async-done(((bf16[208,512]{1,0:T(8,128)(2,1)}), bf16[1664,512]{1,0:T(8,128)(2,1)}) %all-gather.2.cloned.1.call-update) | async-done | bytes 1703952 | tf_op jit(solution)/shard_map/all_gather | solution.py:58
  313.5 1.4 slice-done
  314.9 0.6 convolution_convert_fusion.1
  315.5 0.8 copy.62
  316.3 13.2 %all-to-all-start.4 = ((bf16[4,16,24,128]{3,2,0,1:T(8,128)(2,1)}), bf16[4,16,24,128]{3,2,0,1:T(8,128)(2,1)S(1)}, u32[]{:S(2)}, u32[]{:S(2)}) async-start(bf16[4,16,24,128]{3,2,0,1:T(8,128)(2,1)} %copy.62), calls=%async_computation.5 | async-start | bytes 786432 | tf_op jit(solution)/shard_map/all_to_all | solution.py:139
  329.5 0.1 copy.64
  329.6 18.2 %all-to-all-done.4 = bf16[4,16,24,128]{3,2,0,1:T(8,128)(2,1)S(1)} async-done(((bf16[4,16,24,128]{3,2,0,1:T(8,128)(2,1)}), bf16[4,16,24,128]{3,2,0,1:T(8,128)(2,1)S(1)}, u32[]{:S(2)}, u32[]{:S(2)}) %all-to-all-start.4) | async-done | bytes 393248 | tf_op jit(solution)/shard_map/all_to_all | solution.py:139
  347.8 3.2 gather_fusion.1
  351.1 0.2 fusion.4
  351.3 0.8 fusion
  (60 shorter events, 0.6 us)
Async XLA Ops:
  7.2 69.5 %copy-start.12 = (bf16[128,128]{1,0:T(8,128)(2,1)S(1)}, bf16[128,128]{1,0:T(8,128)(2,1)}, u32[]{:S(2)}) copy-start(bf16[128,128]{1,0:T(8,128)(2,1)} %param.10) | copy-start | bytes 98308
  8.8 67.9 %all-to-all-start.2 = ((f32[16,1,256]{2,1,0:T(1,128)}), f32[16,1,256]{2,1,0:T(1,128)S(1)}, u32[]{:S(2)}, u32[]{:S(2)}) async-start(f32[16,1,256]{2,1,0:T(1,128)} %broadcast_in_dim.6), calls=%async_computation.2 | async-start | bytes 32768 | tf_op jit(solution)/shard_map/all_to_all | solution.py:17
  76.8 0.6 copy-start.10
  77.4 11.7 %copy-start.4 = (f32[64,32,128]{2,1,0:T(8,128)S(1)}, f32[64,32,128]{2,1,0:T(8,128)}, u32[]{:S(2)}) copy-start(f32[64,32,128]{2,1,0:T(8,128)} %param.14) | copy-start | bytes 3145732
  77.4 11.7 %copy-start.5 = (f32[64,32,128]{2,1,0:T(8,128)S(1)}, f32[64,32,128]{2,1,0:T(8,128)}, u32[]{:S(2)}) copy-start(f32[64,32,128]{2,1,0:T(8,128)} %param.15) | copy-start | bytes 3145732
  77.4 11.7 %copy-start.17 = (f32[128]{0:T(128)S(1)}, f32[128]{0:T(128)}, u32[]{:S(2)}) copy-start(f32[128]{0:T(128)} %param.11) | copy-start | bytes 1540
  81.4 31.7 %all-to-all-start.3 = ((bf16[4,16,24,128]{3,2,0,1:T(8,128)(2,1)}), bf16[4,16,24,128]{3,2,0,1:T(8,128)(2,1)S(1)}, u32[]{:S(2)}, u32[]{:S(2)}) async-start(bf16[4,16,24,128]{3,2,0,1:T(8,128)(2,1)} %copy.60), calls=%async_computation.3 | async-start | bytes 786432 | tf_op jit(solution)/shard_map/all_to_all | solution.py:115
  89.4 29.9 %copy-start.15 = (f32[32,128]{1,0:T(8,128)S(1)}, f32[32,128]{1,0:T(8,128)}, u32[]{:S(2)}) copy-start(f32[32,128]{1,0:T(8,128)} %param.19) | copy-start | bytes 49156
  89.4 29.9 %copy-start.13 = (f32[32,128]{1,0:T(8,128)S(1)}, f32[32,128]{1,0:T(8,128)}, u32[]{:S(2)}) copy-start(f32[32,128]{1,0:T(8,128)} %param.17) | copy-start | bytes 49156
  89.4 29.9 %copy-start.14 = (f32[32,128]{1,0:T(8,128)S(1)}, f32[32,128]{1,0:T(8,128)}, u32[]{:S(2)}) copy-start(f32[32,128]{1,0:T(8,128)} %param.18) | copy-start | bytes 49156
  90.6 101.9 %copy-start.11 = (bf16[128,128]{1,0:T(8,128)(2,1)S(1)}, bf16[128,128]{1,0:T(8,128)(2,1)}, u32[]{:S(2)}) copy-start(bf16[128,128]{1,0:T(8,128)(2,1)} %copy-done.10) | copy-start | bytes 98308
  113.2 79.6 %all-to-all-start = ((bf16[64,32,256]{2,1,0:T(8,128)(2,1)}), bf16[64,32,256]{2,1,0:T(8,128)(2,1)S(1)}, u32[]{:S(2)}, u32[]{:S(2)}) async-start(bf16[64,32,256]{2,1,0:T(8,128)(2,1)} %pad_maximum_fusion.1), calls=%async_computation | async-start | bytes 2097152 | tf_op jit(solution)/shard_map/all_to_all | solution.py:46
  119.2 142.4 %reduce-scatter.2.cloned.1.call-start = ((), (), s32[]{:S(2)}) async-start(), calls=%async_computation.6 | async-start | bytes 3620864 | tf_op jit(solution)/shard_map/reduce_scatter | solution.py:128
  192.4 0.7 copy-start.7
  192.4 0.7 copy-start.8
  192.5 158.8 %copy-start.9 = (bf16[512,128]{1,0:T(8,128)(2,1)}, bf16[512,128]{1,0:T(8,128)(2,1)S(1)}, u32[]{:S(2)}) copy-start(bf16[512,128]{1,0:T(8,128)(2,1)S(1)} %get-tuple-element.11) | copy-start | bytes 393220
  193.1 1.0 copy-start
  193.1 1.0 copy-start.1
  196.2 68.6 %copy-start.3 = (f32[64,32,128]{2,1,0:T(8,128)S(1)}, f32[64,32,128]{2,1,0:T(8,128)}, u32[]{:S(2)}) copy-start(f32[64,32,128]{2,1,0:T(8,128)} %param.16) | copy-start | bytes 3145732
  196.3 117.2 %all-gather.2.cloned.1.call-start = ((), (), s32[]{:S(2)}) async-start(), calls=%async_computation.7 | async-start | bytes 1916928 | tf_op jit(solution)/shard_map/all_gather | solution.py:58
  306.7 8.7 %copy-start.6 = (bf16[16,4,32,128]{3,2,0,1:T(8,128)(2,1)}, bf16[16,4,32,128]{3,2,0,1:T(8,128)(2,1)S(1)}, u32[]{:S(2)}) copy-start(bf16[16,4,32,128]{3,2,0,1:T(8,128)(2,1)S(1)} %copy.53) | copy-start | bytes 1572868
  313.5 1.4 slice-start
  313.5 16.0 %copy-start.16 = (f32[128,8]{0,1:T(8,128)S(1)}, f32[128,8]{0,1:T(8,128)}, u32[]{:S(2)}) copy-start(f32[128,8]{0,1:T(8,128)} %param.13) | copy-start | bytes 12292
  316.3 35.0 %copy-start.2 = (bf16[1664,512]{1,0:T(8,128)(2,1)S(1)}, bf16[1664,512]{1,0:T(8,128)(2,1)}, u32[]{:S(2)}) copy-start(bf16[1664,512]{1,0:T(8,128)(2,1)} %all-gather.2.cloned.1.call-done) | copy-start | bytes 5111812
  316.3 31.5 %all-to-all-start.4 = ((bf16[4,16,24,128]{3,2,0,1:T(8,128)(2,1)}), bf16[4,16,24,128]{3,2,0,1:T(8,128)(2,1)S(1)}, u32[]{:S(2)}, u32[]{:S(2)}) async-start(bf16[4,16,24,128]{3,2,0,1:T(8,128)(2,1)} %copy.62), calls=%async_computation.5 | async-start | bytes 786432 | tf_op jit(solution)/shard_map/all_to_all | solution.py:139
Sparse Core Ops, SparseCore 0:
  196.4 65.1 reduce-scatter.1
  264.9 48.4 all-gather.1
where the time goes:
time: 360 us; the launch traced here: 359 us
  blocking collectives  117 us (32%)
  waiting for transfers between devices  113 us (31%)
  starting transfers between devices  70.8 us (20%)
  other arithmetic  24.2 us (7%)
  local copies, waits for them, and re-layouts  17.1 us (5%)
  between operations  14.6 us (4%)
    all_gather x1, blocking collectives, in_one_piece(): lax.all_gather(both, axis, axis=dim, tiled=True)  73 us
    reduce_scatter x1, waiting for transfers between devices, on_device(): lax.psum_scatter(all_terms.astype(jnp.bfloat16), TP, scatter_dimension=0,...  65.2 us
    all_to_all x1, starting transfers between devices, copy_for_each(): lax.all_to_all(jnp.broadcast_to(array[None], (size, *array.shape)), axis,...  43.7 us
    all_to_all x1, blocking collectives, on_device(): lax.all_to_all(down_new, 'fs', split_axis=0, concat_axis=1, tiled=True)  41.8 us
    all_to_all x1, waiting for transfers between devices, on_device(): lax.all_to_all(outgoing, 'fs', split_axis=1, concat_axis=1, tiled=True)  22.6 us
    another operation x3, other arithmetic  18.2 us
    all_to_all x1, waiting for transfers between devices, on_device(): lax.all_to_all(outputs.reshape(experts_here, shard_count, CAPACITY, slice...  18.2 us
    all_to_all x1, starting transfers between devices, on_device(): lax.all_to_all(outputs.reshape(experts_here, shard_count, CAPACITY, slice...  13.2 us
  transfers between devices with their start and end apart: 6, of which 4 were waited for; matrix products, arithmetic and copies ran while one was open for 7% of the time, Pallas kernels for 0%

commit v1 on v0

v1 whole, which is shorter than its diff:
```python
import functools

import jax
import jax.numpy as jnp
from jax import lax
from jax.experimental import pallas as pl
from jax.experimental.pallas import tpu as pltpu
from jax.sharding import PartitionSpec as P

CAPACITY = 24
NORM_EPS = 1e-05
ROUTED_SCALE = 2.5
MESH = pl.DeviceIdType.MESH
F32 = jnp.float32
BF16 = jnp.bfloat16


def nt_dot(a, b):
    return lax.dot_general(a, b, (((1,), (1,)), ((), ())), preferred_element_type=F32)


def nn_dot(a, b):
    return jnp.dot(a, b, preferred_element_type=F32)


def layer_kernel(
    nz, nt, full_width,
    tok_ref, gain_ref, ids_ref, score_ref, gate_ref, up_ref, down_ref, sg_ref, su_ref, sd_ref,
    o1, o2, osh, out_ref,
    w1, w2, ws, stat, xs, xr, own, pdo, pdr, q, rr, h, rb, rt, sel_hi, sel_lo, nrm_ref,
    st_s, st_r, tk_s, tk_r, w1_s, w1_r, f1_s, f1_r, w2_s, w2_r, f2_s, f2_r, sh_s, sh_r, fs_s, fs_r,
    dd_s, dd_r, rs_s, rs_r, ag_s, ag_r, fw_s, fw_r, re_s, re_r,
):
    z = lax.axis_index("fs")
    t = lax.axis_index("tp")
    g = lax.axis_index("grp")
    y = lax.rem(g, 2)
    mate = g + 1 - 2 * y
    core = lax.rem(t, 2)
    x = t // 2
    nx = nt // 2
    twin = t + 1 - 2 * core

    experts, ff_here, width = gate_ref.shape
    eh = experts // nz
    ff = ff_here * nz
    half = ff // 2
    toks = tok_ref.shape[0]
    cap_rows = nz * CAPACITY
    seg = cap_rows // nx
    sseg = toks // nx
    units = eh + 1

    def unit_rows(u):
        return (u * seg, seg) if u < eh else (eh * seg, sseg)

    def rcopy(src, dst, ss, rs, **where):
        return pltpu.make_async_remote_copy(
            src_ref=src, dst_ref=dst, send_sem=ss, recv_sem=rs, device_id=where, device_id_type=MESH
        )

    def each(n, me, body):
        def step(k, carry):
            body(lax.rem(me + k, n))
            return carry

        lax.fori_loop(1, n, step, 0)

    barrier = pltpu.get_barrier_semaphore()
    each(nz, z, lambda d: pl.semaphore_signal(barrier, inc=1, device_id={"fs": d}, device_id_type=MESH))
    each(nt, t, lambda d: pl.semaphore_signal(barrier, inc=1, device_id={"tp": d}, device_id_type=MESH))
    pl.semaphore_signal(barrier, inc=1, device_id={"grp": mate}, device_id_type=MESH)

    gain = gain_ref[...]
    w1[0] = (gate_ref[...] * gain[None]).astype(BF16)
    w1[1] = (up_ref[...] * gain[None]).astype(BF16)
    w2[...] = down_ref[...].astype(BF16)
    hr = ff_here // 2
    ws[0] = (sg_ref[...] * gain).astype(BF16).reshape(2, hr, width)
    ws[1] = (su_ref[...] * gain).astype(BF16).reshape(2, hr, width)
    ws[2] = sd_ref[...].astype(BF16).reshape(2, hr, width)
    rows_z = pl.ds(pl.multiple_of(z * ff_here, ff_here), ff_here)
    o1[y, :, rows_z, :] = w1[y, pl.ds(eh * z, eh)]
    o2[pl.ds(2 * y, 2), rows_z, :] = w2[pl.ds(eh * z + 2 * y, 2)]
    osh[:, z, y] = ws[:, y]

    tok_t = tok_ref[...].astype(F32).T
    stat[t] = jnp.concatenate(
        [
            jnp.sum(tok_t, axis=0, keepdims=True),
            jnp.sum(tok_t * tok_t, axis=0, keepdims=True),
            jnp.zeros((6, toks), F32),
        ],
        axis=0,
    )

    pl.semaphore_wait(barrier, nz + nt - 1)

    def stat_copy(src, dst):
        return rcopy(stat.at[src], stat.at[src], st_s.at[dst], st_r.at[src], tp=dst)

    each(nt, t, lambda d: stat_copy(t, d).start())

    def w1_copy(e, src, dst):
        return rcopy(
            w1.at[y, eh * dst + e],
            o1.at[y, e, pl.ds(pl.multiple_of(src * ff_here, ff_here), ff_here), :],
            w1_s.at[e, dst], w1_r.at[e, src], fs=dst,
        )

    def w2_copy(src, dst):
        return rcopy(
            w2.at[pl.ds(eh * dst + 2 * y, 2)],
            o2.at[pl.ds(2 * y, 2), pl.ds(pl.multiple_of(src * ff_here, ff_here), ff_here), :],
            w2_s.at[dst], w2_r.at[src], fs=dst,
        )

    def sh_copy(src, dst):
        return rcopy(ws.at[:, y], osh.at[:, src, y], sh_s.at[dst], sh_r.at[src], fs=dst)

    def tk_copy(src, dst):
        return rcopy(xs.at[dst], xr.at[src], tk_s.at[dst], tk_r.at[src], fs=dst)

    each(nz, z, lambda d: w1_copy(0, z, d).start())

    ids = ids_ref[...]
    scores = score_ref[...]
    weight = scores / jnp.sum(scores, axis=1, keepdims=True) * ROUTED_SCALE
    lane = lax.broadcasted_iota(jnp.int32, (toks, 128), 1)
    chosen = jnp.zeros((toks, 128), F32)
    spread = jnp.zeros((toks, 128), F32)
    for k in range(ids.shape[1]):
        hit = ids[:, k : k + 1] == lane
        chosen = chosen + jnp.where(hit, 1.0, 0.0)
        spread = spread + jnp.where(hit, weight[:, k : k + 1], 0.0)
    below = lax.broadcasted_iota(jnp.int32, (toks, toks), 1) < lax.broadcasted_iota(
        jnp.int32, (toks, toks), 0
    )
    rank = nn_dot(jnp.where(below, 1.0, 0.0).astype(BF16), chosen.astype(BF16))
    rank = jnp.where(chosen > 0.5, rank, -1.0)
    rank_t = rank.T[:experts]
    slot = lax.broadcasted_iota(jnp.int32, (experts, CAPACITY, toks), 1).astype(F32)
    pick = jnp.where(rank_t[:, None, :] == slot, 1.0, 0.0).reshape(experts * CAPACITY, toks)
    pick = pick.astype(BF16)

    each(nt, t, lambda d: stat_copy(d, t).wait_recv())
    total = jnp.sum(stat[...], axis=0)
    mean = total[0:1] / full_width
    var = total[1:2] / full_width - mean * mean
    nrm = ((tok_t - mean) * lax.rsqrt(var + NORM_EPS)).T.astype(BF16)
    nrm_ref[...] = nrm
    xs[...] = nn_dot(pick, nrm).astype(BF16).reshape(nz, eh * CAPACITY, width)
    each(nz, z, lambda d: tk_copy(z, d).start())
    for e in range(1, eh):
        each(nz, z, lambda d: w1_copy(e, z, d).start())
    each(nz, z, lambda d: sh_copy(z, d).start())
    each(nz, z, lambda d: w2_copy(z, d).start())

    xr[z] = xs[z]
    row = lax.broadcasted_iota(jnp.int32, (128, experts * CAPACITY), 0) * CAPACITY
    col = lax.broadcasted_iota(jnp.int32, (128, experts * CAPACITY), 1)
    wide = jnp.where((col >= row) & (col < row + CAPACITY), 1.0, 0.0).astype(BF16)
    colf = col[:toks].astype(F32)
    col_slot = colf - jnp.floor((colf + 0.5) * (1.0 / CAPACITY)) * CAPACITY
    mine = nn_dot(rank.astype(BF16), wide) == col_slot
    hi = spread.astype(BF16)
    lo = (spread - hi.astype(F32)).astype(BF16)
    sel_hi[...] = jnp.where(mine, nn_dot(hi, wide), 0.0).astype(BF16)
    sel_lo[...] = jnp.where(mine, nn_dot(lo, wide), 0.0).astype(BF16)

    def f1_copy(e, side):
        return rcopy(o1.at[side, e], o1.at[side, e], f1_s.at[e], f1_r.at[e], grp=mate)

    def f2_copy(side):
        part = o2.at[pl.ds(2 * side, 2)]
        return rcopy(part, part, f2_s, f2_r, grp=mate)

    def fs_copy(side):
        return rcopy(osh.at[:, :, side], osh.at[:, :, side], fs_s, fs_r, grp=mate)

    def dd_copy(u):
        r0, n = unit_rows(u)
        rows = pl.ds(nx * r0, nx * n)
        return rcopy(pdo.at[rows], pdr.at[rows], dd_s.at[u], dd_r.at[u], tp=twin)

    def rs_copy(u, src, dst):
        r0, n = unit_rows(u)
        rows = pl.ds(r0, n)
        return rcopy(q.at[dst, rows], rr.at[src, rows], rs_s.at[u, dst], rs_r.at[u, src], tp=2 * dst + core)

    def ag_copy(u, src, dst):
        r0, n = unit_rows(u)
        part = h.at[core, src, pl.ds(r0, n)]
        return rcopy(part, part, ag_s.at[u, dst], ag_r.at[u, src], tp=2 * dst + core)

    def fw_copy(u, src, side):
        r0, n = unit_rows(u)
        part = h.at[side, src, pl.ds(r0, n)]
        return rcopy(part, part, fw_s.at[u, src], fw_r.at[u, src], tp=twin)

    def re_copy(p, src, dst):
        rows = pl.ds(2 * CAPACITY * p, 2 * CAPACITY)
        return rcopy(rb.at[dst, rows], rt.at[src, rows], re_s.at[p, dst], re_r.at[p, src], fs=dst)

    def paired(u, part):
        cols = pl.ds(pl.multiple_of(part * half, half), half)
        if u < eh:
            return jnp.concatenate([o1[0, u, cols, :], o1[1, u, cols, :]], axis=0)
        zs = pl.ds(part * (nz // 2), nz // 2)
        return jnp.concatenate(
            [osh[0, zs].reshape(half, width), osh[1, zs].reshape(half, width)], axis=0
        )

    def first_matmul(u):
        r0, n = unit_rows(u)
        if u < eh:
            arrived = xr[...].astype(F32)[:, u * CAPACITY : (u + 1) * CAPACITY, :]
            rows_in = arrived.reshape(cap_rows, width).astype(BF16)
        else:
            rows_in = nrm_ref[...]
        pdo[nx * r0 : nx * (r0 + n), :] = nt_dot(rows_in, paired(u, 1 - core)).astype(BF16)
        dd_copy(u).start()
        own[nx * r0 : nx * (r0 + n), :] = nt_dot(rows_in, paired(u, core))

    def chip_sum(u):
        r0, n = unit_rows(u)
        rows = slice(nx * r0, nx * (r0 + n))
        dd_copy(u).wait_recv()
        both = own[rows, :] + pdr[rows, :].astype(F32)
        q[:, r0 : r0 + n, :] = both.astype(BF16).reshape(nx, n, 2 * half)
        each(nx, x, lambda d: rs_copy(u, x, d).start())
        rr[x, r0 : r0 + n, :] = q[x, r0 : r0 + n, :]

    def activate(u):
        r0, n = unit_rows(u)
        each(nx, x, lambda d: rs_copy(u, d, x).wait_recv())
        pre = jnp.sum(rr[:, r0 : r0 + n, :].astype(F32), axis=0)
        h[core, x, r0 : r0 + n, :] = (jax.nn.silu(pre[:, :half]) * pre[:, half:]).astype(BF16)
        each(nx, x, lambda d: ag_copy(u, x, d).start())
        fw_copy(u, x, core).start()

    def pass_on(u):
        def one(d):
            ag_copy(u, d, x).wait_recv()
            fw_copy(u, d, core).start()

        each(nx, x, one)

    def hidden_part(u, part):
        r0, n = unit_rows(u)
        return h[part, :, r0 : r0 + n, :].reshape(nx * n, half)

    def all_hidden(u):
        def one(k, carry):
            fw_copy(u, k, 1 - core).wait_recv()
            return carry

        lax.fori_loop(0, nx, one, 0)

    def arrivals(e):
        each(nz, z, lambda d: w1_copy(e, d, z).wait_recv())
        f1_copy(e, y).start()

    arrivals(0)
    each(nz, z, lambda d: tk_copy(d, z).wait_recv())
    for e in range(eh):
        f1_copy(e, 1 - y).wait_recv()
        first_matmul(e)
        if e + 1 < eh:
            arrivals(e + 1)
        chip_sum(e)
    each(nz, z, lambda d: sh_copy(d, z).wait_recv())
    fs_copy(y).start()
    each(nz, z, lambda d: w2_copy(d, z).wait_recv())
    f2_copy(y).start()
    fs_copy(1 - y).wait_recv()
    first_matmul(eh)
    chip_sum(eh)
    for u in range(units):
        activate(u)
        if u > 0:
            pass_on(u - 1)
    pass_on(units - 1)
    f2_copy(1 - y).wait_recv()
    for p in range(eh // 2):
        both = []
        for u in (2 * p, 2 * p + 1):
            all_hidden(u)
            res = nn_dot(hidden_part(u, 0), o2[u, :half, :]) + nn_dot(hidden_part(u, 1), o2[u, half:, :])
            both.append(res.reshape(nz, CAPACITY, width))
        rb[:, 2 * CAPACITY * p : 2 * CAPACITY * (p + 1), :] = jnp.concatenate(both, axis=1).astype(BF16)
        each(nz, z, lambda d: re_copy(p, z, d).start())
    rt[z] = rb[z]
    all_hidden(eh)
    down = osh[2].reshape(ff, width)
    shared = nn_dot(hidden_part(eh, 0), down[:half]) + nn_dot(hidden_part(eh, 1), down[half:])
    for p in range(eh // 2):
        each(nz, z, lambda d: re_copy(p, d, z).wait_recv())
    back = rt[...].reshape(experts * CAPACITY, width)
    out_ref[...] = (nn_dot(sel_hi[...], back) + nn_dot(sel_lo[...], back) + shared).astype(BF16)

    each(nt, t, lambda d: stat_copy(t, d).wait_send())
    each(nz, z, lambda d: tk_copy(z, d).wait_send())
    for e in range(eh):
        each(nz, z, lambda d: w1_copy(e, z, d).wait_send())
        f1_copy(e, y).wait_send()
    each(nz, z, lambda d: w2_copy(z, d).wait_send())
    f2_copy(y).wait_send()
    each(nz, z, lambda d: sh_copy(z, d).wait_send())
    fs_copy(y).wait_send()
    for u in range(units):
        dd_copy(u).wait_send()
        each(nx, x, lambda d: rs_copy(u, x, d).wait_send())
        each(nx, x, lambda d: ag_copy(u, x, d).wait_send())
        fw_copy(u, x, core).wait_send()
        each(nx, x, lambda d: fw_copy(u, d, core).wait_send())
    for p in range(eh // 2):
        each(nz, z, lambda d: re_copy(p, z, d).wait_send())


def on_device(nz, nt, tokens, norm_gain, expert_ids, route_scores, gate, up, down, sg, su, sd):
    experts, ff_here, width = gate.shape
    eh = experts // nz
    ff = ff_here * nz
    half = ff // 2
    toks = tokens.shape[0]
    nx = nt // 2
    rows = eh * nz * CAPACITY + toks
    disp = (nz, eh * CAPACITY, width)
    units = eh + 1
    vmem = pl.BlockSpec(memory_space=pltpu.VMEM)
    dma = pltpu.SemaphoreType.DMA
    pairs = eh // 2
    sems = []
    for shape in (
        (nt,), (nz,), (eh, nz), (eh,), (nz,), (), (nz,), (), (units,), (units, nx), (units, nx), (units, nx), (pairs, nz),
    ):
        sems += [dma(shape), dma(shape)]
    o1, o2, osh, out = pl.pallas_call(
        functools.partial(layer_kernel, nz, nt, width * nt),
        out_shape=(
            jax.ShapeDtypeStruct((2, eh, ff, width), BF16),
            jax.ShapeDtypeStruct((eh, ff, width), BF16),
            jax.ShapeDtypeStruct((3, nz, 2, ff_here // 2, width), BF16),
            jax.ShapeDtypeStruct((toks, width), BF16),
        ),
        in_specs=[vmem] * 10,
        out_specs=(vmem,) * 4,
        scratch_shapes=[
            pltpu.VMEM((2, experts, ff_here, width), BF16),
            pltpu.VMEM((experts, ff_here, width), BF16),
            pltpu.VMEM((3, 2, ff_here // 2, width), BF16),
            pltpu.VMEM((nt, 8, toks), F32),
            pltpu.VMEM(disp, BF16),
            pltpu.VMEM(disp, BF16),
            pltpu.VMEM((rows, 2 * half), F32),
            pltpu.VMEM((rows, 2 * half), BF16),
            pltpu.VMEM((rows, 2 * half), BF16),
            pltpu.VMEM((nx, rows // nx, 2 * half), BF16),
            pltpu.VMEM((nx, rows // nx, 2 * half), BF16),
            pltpu.VMEM((2, nx, rows // nx, half), BF16),
            pltpu.VMEM(disp, BF16),
            pltpu.VMEM(disp, BF16),
            pltpu.VMEM((toks, experts * CAPACITY), BF16),
            pltpu.VMEM((toks, experts * CAPACITY), BF16),
            pltpu.VMEM((toks, width), BF16),
            *sems,
        ],
        compiler_params=pltpu.CompilerParams(
            collective_id=0, has_side_effects=True, vmem_limit_bytes=56 * 1024 * 1024
        ),
        name="layer",
    )(tokens, norm_gain.reshape(1, width), expert_ids, route_scores, gate, up, down, sg, su, sd)
    osh = osh.reshape(3, ff, width)
    return o1[0], o1[1], o2, osh[0], osh[1], osh[2], out


def solution(mesh):
    return jax.shard_map(
        functools.partial(on_device, mesh.shape["fs"], mesh.shape["tp"]),
        mesh=mesh,
        in_specs=(
            P(("grp", "fs"), "tp"),
            P("tp"),
            P(("grp", "fs"), None),
            P(("grp", "fs"), None),
            P(None, "fs", "tp"),
            P(None, "fs", "tp"),
            P(None, "fs", "tp"),
            P("fs", "tp"),
            P("fs", "tp"),
            P("fs", "tp"),
        ),
        out_specs=(
            P(("grp", "fs"), None, "tp"),
            P(("grp", "fs"), None, "tp"),
            P(("grp", "fs"), None, "tp"),
            P("grp", "tp"),
            P("grp", "tp"),
            P("grp", "tp"),
            P(("grp", "fs"), "tp"),
        ),
        check_vma=False,
    )
```

time: 360 us -> 182 us (0.51)
  the two profiles are of different devices: /device:TPU:66 before, /device:TPU:65 now
where the time goes in v1:
time: 182 us
  Pallas kernels  174 us (96%)
  local copies, waits for them, and re-layouts  7.04 us (4%)
    pallas_call x1, Pallas kernels, on_device(): pl.pallas_call(functools.partial(layer_kernel, nz, nt, width * nt), out_s...  174 us
    unnamed x12, local copies, waits for them, and re-layouts  4 us

profile of v1, /device:TPU:65, one launch (start us, length us, event | category | flops | bytes accessed | tf_op | source)
XLA Modules:
  0.0 181.7 jit_solution(4563400575988914015)
XLA Ops:
  0.6 0.0 copy-start.3
  0.6 1.4 copy.17.ids_ref
  2.1 0.0 copy-done.3
  2.1 0.7 copy.18.score_ref
  2.8 174.0 %layer.1 = (bf16[2,4,512,128]{3,2,1,0:T(8,128)(2,1)}, bf16[4,512,128]{2,1,0:T(8,128)(2,1)}, bf16[3,16,2,16,128]{4,3,2,1,0:T(8,128)(2,1)}, bf16[128,128]{1,0:T(8,128)(2,1)}) custom-call(bf16[128,128]{1,0:T(8,128)(2,1)} %tok_ref.1, f32[1,128]{1,0:T(1,128)} %bitcast.11, s32[128,8]{1,0:T(8,128)} %copy.17.ids_ref, f32[128,8]{1,0:T(8,128)} %copy.18.score_ref, ...), custom_call_target="tpu_custom_call" | custom-call | tf_op jit(solution)/shard_map/layer/pallas_call | solution.py:339
  176.8 0.0 copy-start.1
  176.8 2.3 %slice_bitcast_fusion = (bf16[4,512,128]{2,1,0:T(8,128)(2,1)}, bf16[4,512,128]{2,1,0:T(8,128)(2,1)}) fusion(bf16[2,4,512,128]{3,2,1,0:T(8,128)(2,1)} %get-tuple-element.11), kind=kLoop, calls=%fused_computation | loop fusion | bytes 2097152 | tf_op jit(solution)/shard_map/squeeze | solution.py:375
  179.1 0.0 copy-start
  179.1 0.0 copy-done.1
  179.1 0.8 fusion
  179.9 0.4 copy-done
  180.3 0.0 copy-start.2
  180.3 0.8 copy.21
  181.1 0.0 copy-done.2
  181.1 0.6 copy.22
Async XLA Ops:
  0.6 1.4 copy-start.3
  176.8 2.3 %copy-start.1 = (bf16[3,16,2,16,128]{4,3,2,1,0:T(8,128)(2,1)S(1)}, bf16[3,16,2,16,128]{4,3,2,1,0:T(8,128)(2,1)}, u32[]{:S(2)}) copy-start(bf16[3,16,2,16,128]{4,3,2,1,0:T(8,128)(2,1)} %get-tuple-element.13) | copy-start | bytes 1179652
  179.1 1.2 copy-start
  180.3 0.8 copy-start.2

commit v2 on v1

v2 whole, which is shorter than its diff:
```python
import functools

import jax
import jax.numpy as jnp
from jax import lax
from jax.experimental import pallas as pl
from jax.experimental.pallas import tpu as pltpu
from jax.sharding import PartitionSpec as P

CAPACITY = 24
NORM_EPS = 1e-05
ROUTED_SCALE = 2.5
MESH = pl.DeviceIdType.MESH
F32 = jnp.float32
BF16 = jnp.bfloat16


def nt_dot(a, b):
    return lax.dot_general(a, b, (((1,), (1,)), ((), ())), preferred_element_type=F32)


def nn_dot(a, b):
    return jnp.dot(a, b, preferred_element_type=F32)


def layer_kernel(
    nz, nt, full_width,
    tok_ref, gain_ref, ids_ref, score_ref, gate_hbm, up_hbm, down_hbm, sg_ref, su_ref, sd_ref,
    og_hbm, ou_hbm, od_hbm, osg_hbm, osu_hbm, osd_hbm, out_ref,
    gate_ref, up_ref, down_ref, og, ou, o2, osg, osu, osd, in_sem, out_sem,
    osh, w1, w2, ws, stat, xs, xr, own, pdo, pdr, q, rr, h, rb, rt, sel_hi, sel_lo, nrm_ref,
    st_s, st_r, tk_s, tk_r, w1_s, w1_r, f1_s, f1_r, w2_s, w2_r, f2_s, f2_r, sh_s, sh_r, fs_s, fs_r,
    dd_s, dd_r, rs_s, rs_r, ag_s, ag_r, fw_s, fw_r, re_s, re_r,
):
    z = lax.axis_index("fs")
    t = lax.axis_index("tp")
    g = lax.axis_index("grp")
    y = lax.rem(g, 2)
    mate = g + 1 - 2 * y
    core = lax.rem(t, 2)
    x = t // 2
    nx = nt // 2
    twin = t + 1 - 2 * core
    ahead = 1 - 2 * core
    n_long = nx // 2
    n_short = nx - 1 - n_long
    o1 = (og, ou)

    experts, ff_here, width = gate_hbm.shape
    eh = experts // nz
    ff = ff_here * nz
    half = ff // 2
    toks = tok_ref.shape[0]
    cap_rows = nz * CAPACITY
    seg = cap_rows // nx
    sseg = toks // nx
    units = eh + 1

    def unit_rows(u):
        return (u * seg, seg) if u < eh else (eh * seg, sseg)

    def rcopy(src, dst, ss, rs, **where):
        return pltpu.make_async_remote_copy(
            src_ref=src, dst_ref=dst, send_sem=ss, recv_sem=rs, device_id=where, device_id_type=MESH
        )

    def each(n, me, body):
        def step(k, carry):
            body(lax.rem(me + k, n))
            return carry

        lax.fori_loop(1, n, step, 0)

    barrier = pltpu.get_barrier_semaphore()
    each(nz, z, lambda d: pl.semaphore_signal(barrier, inc=1, device_id={"fs": d}, device_id_type=MESH))
    each(nt, t, lambda d: pl.semaphore_signal(barrier, inc=1, device_id={"tp": d}, device_id_type=MESH))
    pl.semaphore_signal(barrier, inc=1, device_id={"grp": mate}, device_id_type=MESH)

    loads = [
        pltpu.make_async_copy(src, dst, in_sem.at[i])
        for i, (src, dst) in enumerate(((gate_hbm, gate_ref), (up_hbm, up_ref), (down_hbm, down_ref)))
    ]
    for load in loads:
        load.start()
    stores = [
        pltpu.make_async_copy(src, dst, out_sem.at[i])
        for i, (src, dst) in enumerate(
            ((og, og_hbm), (ou, ou_hbm), (o2, od_hbm), (osg, osg_hbm), (osu, osu_hbm), (osd, osd_hbm))
        )
    ]
    gain = gain_ref[...]
    hr = ff_here // 2
    ws[0] = (sg_ref[...] * gain).astype(BF16).reshape(2, hr, width)
    ws[1] = (su_ref[...] * gain).astype(BF16).reshape(2, hr, width)
    ws[2] = sd_ref[...].astype(BF16).reshape(2, hr, width)
    loads[0].wait()
    w1[0] = (gate_ref[...] * gain[None]).astype(BF16)
    loads[1].wait()
    w1[1] = (up_ref[...] * gain[None]).astype(BF16)
    loads[2].wait()
    w2[...] = down_ref[...].astype(BF16)
    rows_z = pl.ds(pl.multiple_of(z * ff_here, ff_here), ff_here)

    def on_side(body):
        for side in (0, 1):
            pl.when(y == side)(functools.partial(body, side))

    def keep_own(side):
        o1[side][:, rows_z, :] = w1[side, pl.ds(eh * z, eh)]

    on_side(keep_own)
    o2[pl.ds((eh // 2) * y, eh // 2), rows_z, :] = w2[pl.ds(eh * z + (eh // 2) * y, eh // 2)]
    osh[:, z, y] = ws[:, y]

    tok_t = tok_ref[...].astype(F32).T
    stat[t] = jnp.concatenate(
        [
            jnp.sum(tok_t, axis=0, keepdims=True),
            jnp.sum(tok_t * tok_t, axis=0, keepdims=True),
            jnp.zeros((6, toks), F32),
        ],
        axis=0,
    )

    pl.semaphore_wait(barrier, nz + nt - 1)

    def stat_copy(src, dst):
        return rcopy(stat.at[src], stat.at[src], st_s.at[dst], st_r.at[src], tp=dst)

    each(nt, t, lambda d: stat_copy(t, d).start())

    def w1_copy(side, e, src, dst):
        return rcopy(
            w1.at[side, eh * dst + e],
            o1[side].at[e, pl.ds(pl.multiple_of(src * ff_here, ff_here), ff_here), :],
            w1_s.at[e, dst], w1_r.at[e, src], fs=dst,
        )

    def w2_copy(j, src, dst):
        return rcopy(
            w2.at[eh * dst + (eh // 2) * y + j],
            o2.at[(eh // 2) * y + j, pl.ds(pl.multiple_of(src * ff_here, ff_here), ff_here), :],
            w2_s.at[j, dst], w2_r.at[j, src], fs=dst,
        )

    def sh_copy(src, dst):
        return rcopy(ws.at[:, y], osh.at[:, src, y], sh_s.at[dst], sh_r.at[src], fs=dst)

    def tk_copy(src, dst):
        return rcopy(xs.at[dst], xr.at[src], tk_s.at[dst], tk_r.at[src], fs=dst)

    def send_w1(first, last):
        def one(side):
            for e in range(first, last):
                each(nz, z, lambda d: w1_copy(side, e, z, d).start())

        on_side(one)

    send_w1(0, 1)

    ids = ids_ref[...]
    scores = score_ref[...]
    weight = scores / jnp.sum(scores, axis=0, keepdims=True) * ROUTED_SCALE
    expert = lax.broadcasted_iota(jnp.int32, (experts, toks), 0)
    chosen = jnp.zeros((experts, toks), F32)
    spread = jnp.zeros((experts, toks), F32)
    for k in range(ids.shape[0]):
        hit = ids[k : k + 1] == expert
        chosen = chosen + jnp.where(hit, 1.0, 0.0)
        spread = spread + jnp.where(hit, weight[k : k + 1], 0.0)
    above = lax.broadcasted_iota(jnp.int32, (toks, toks), 0) < lax.broadcasted_iota(
        jnp.int32, (toks, toks), 1
    )
    rank_t = nn_dot(chosen.astype(BF16), jnp.where(above, 1.0, 0.0).astype(BF16))
    rank_t = jnp.where(chosen > 0.5, rank_t, -1.0)
    slot = lax.broadcasted_iota(jnp.int32, (experts, CAPACITY, toks), 1).astype(F32)
    pick = jnp.where(rank_t[:, None, :] == slot, 1.0, 0.0).reshape(experts * CAPACITY, toks)
    pick = pick.astype(BF16)

    each(nt, t, lambda d: stat_copy(d, t).wait_recv())
    total = jnp.sum(stat[...], axis=0)
    mean = total[0:1] / full_width
    var = total[1:2] / full_width - mean * mean
    nrm = ((tok_t - mean) * lax.rsqrt(var + NORM_EPS)).T.astype(BF16)
    nrm_ref[...] = nrm
    xs[...] = nn_dot(pick, nrm).astype(BF16).reshape(nz, eh * CAPACITY, width)
    each(nz, z, lambda d: tk_copy(z, d).start())
    send_w1(1, eh)
    each(nz, z, lambda d: sh_copy(z, d).start())
    for j in range(eh // 2):
        each(nz, z, lambda d: w2_copy(j, z, d).start())

    xr[z] = xs[z]
    rank = jnp.concatenate([rank_t, jnp.full((toks - experts, toks), -1.0, F32)], axis=0).T
    spread = jnp.concatenate([spread, jnp.zeros((toks - experts, toks), F32)], axis=0).T
    row = lax.broadcasted_iota(jnp.int32, (toks, experts * CAPACITY), 0) * CAPACITY
    col = lax.broadcasted_iota(jnp.int32, (toks, experts * CAPACITY), 1)
    wide = jnp.where((col >= row) & (col < row + CAPACITY), 1.0, 0.0).astype(BF16)
    colf = col.astype(F32)
    col_slot = colf - jnp.floor((colf + 0.5) * (1.0 / CAPACITY)) * CAPACITY
    mine = nn_dot(rank.astype(BF16), wide) == col_slot
    hi = spread.astype(BF16)
    lo = (spread - hi.astype(F32)).astype(BF16)
    sel_hi[...] = jnp.where(mine, nn_dot(hi, wide), 0.0).astype(BF16)
    sel_lo[...] = jnp.where(mine, nn_dot(lo, wide), 0.0).astype(BF16)

    def f1_copy(e, side):
        return rcopy(o1[side].at[e], o1[side].at[e], f1_s.at[e], f1_r.at[e], grp=mate)

    def f2_copy(j, side):
        part = o2.at[(eh // 2) * side + j]
        return rcopy(part, part, f2_s.at[j], f2_r.at[j], grp=mate)

    def fs_copy(side):
        return rcopy(osh.at[:, :, side], osh.at[:, :, side], fs_s, fs_r, grp=mate)

    def dd_copy(u):
        r0, n = unit_rows(u)
        rows = pl.ds(nx * r0, nx * n)
        return rcopy(pdo.at[rows], pdr.at[rows], dd_s.at[u], dd_r.at[u], tp=twin)

    def turn(k):
        return lax.rem(x + k * ahead + nx, nx)

    def rs_copy(u, arm, k):
        r0, n = unit_rows(u)
        rows = pl.ds(r0, n)
        goal, near, i = (turn(n_long - k), turn(1), k) if arm == 0 else (turn(k - n_short), turn(-1), n_long + k)
        return rcopy(q.at[goal, rows], rr.at[i, rows], rs_s.at[u, i], rs_r.at[u, i], tp=2 * near + core)

    def ag_copy(u, src, dst):
        r0, n = unit_rows(u)
        part = h.at[core, src, pl.ds(r0, n)]
        return rcopy(part, part, ag_s.at[u, dst], ag_r.at[u, src], tp=2 * dst + core)

    def fw_copy(u, src, side):
        r0, n = unit_rows(u)
        part = h.at[side, src, pl.ds(r0, n)]
        return rcopy(part, part, fw_s.at[u, src], fw_r.at[u, src], tp=twin)

    def re_copy(u, src, dst):
        rows = pl.ds(CAPACITY * u, CAPACITY)
        return rcopy(rb.at[dst, rows], rt.at[src, rows], re_s.at[u, dst], re_r.at[u, src], fs=dst)

    def paired(u, part):
        cols = pl.ds(pl.multiple_of(part * half, half), half)
        if u < eh:
            return jnp.concatenate([og[u, cols, :], ou[u, cols, :]], axis=0)
        zs = pl.ds(part * (nz // 2), nz // 2)
        return jnp.concatenate(
            [osh[0, zs].reshape(half, width), osh[1, zs].reshape(half, width)], axis=0
        )

    def first_matmul(u):
        r0, n = unit_rows(u)
        if u < eh:
            arrived = xr[...].astype(F32)[:, u * CAPACITY : (u + 1) * CAPACITY, :]
            rows_in = arrived.reshape(cap_rows, width).astype(BF16)
        else:
            rows_in = nrm_ref[...]
        pdo[nx * r0 : nx * (r0 + n), :] = nt_dot(rows_in, paired(u, 1 - core)).astype(BF16)
        dd_copy(u).start()
        own[nx * r0 : nx * (r0 + n), :] = nt_dot(rows_in, paired(u, core))

    def chip_sum(u):
        r0, n = unit_rows(u)
        rows = slice(nx * r0, nx * (r0 + n))
        dd_copy(u).wait_recv()
        both = own[rows, :] + pdr[rows, :].astype(F32)
        q[:, r0 : r0 + n, :] = both.astype(BF16).reshape(nx, n, 2 * half)
        rs_copy(u, 0, 0).start()
        rs_copy(u, 1, 0).start()

    def rs_step(u, k):
        r0, n = unit_rows(u)
        rows = slice(r0, r0 + n)
        for arm, steps in ((0, n_long), (1, n_short)):
            if k < steps:
                rs_copy(u, arm, k - 1).wait_recv()
                goal, i = (turn(n_long - k), k - 1) if arm == 0 else (turn(k - n_short), n_long + k - 1)
                q[goal, rows, :] = (q[goal, rows, :].astype(F32) + rr[i, rows, :].astype(F32)).astype(BF16)
                rs_copy(u, arm, k).start()

    def activate(u):
        r0, n = unit_rows(u)
        rows = slice(r0, r0 + n)
        rs_copy(u, 0, n_long - 1).wait_recv()
        rs_copy(u, 1, n_short - 1).wait_recv()
        pre = q[x, rows, :].astype(F32) + rr[n_long - 1, rows, :].astype(F32) + rr[nx - 2, rows, :].astype(F32)
        h[core, x, r0 : r0 + n, :] = (jax.nn.silu(pre[:, :half]) * pre[:, half:]).astype(BF16)
        each(nx, x, lambda d: ag_copy(u, x, d).start())
        fw_copy(u, x, core).start()

    def pass_on(u):
        def one(d):
            ag_copy(u, d, x).wait_recv()
            fw_copy(u, d, core).start()

        each(nx, x, one)

    def hidden_part(u, part):
        r0, n = unit_rows(u)
        return h[part, :, r0 : r0 + n, :].reshape(nx * n, half)

    def all_hidden(u):
        def one(k, carry):
            fw_copy(u, k, 1 - core).wait_recv()
            return carry

        lax.fori_loop(0, nx, one, 0)

    def arrivals(u):
        def one(side):
            each(nz, z, lambda d: w1_copy(side, u, d, z).wait_recv())
            f1_copy(u, side).start()

        if u < eh:
            on_side(one)
        else:
            each(nz, z, lambda d: sh_copy(d, z).wait_recv())
            fs_copy(y).start()

    def passed(u):
        if u < eh:
            on_side(lambda side: f1_copy(u, 1 - side).wait_recv())
        else:
            fs_copy(1 - y).wait_recv()

    order = tuple(range(units))
    arrivals(order[0])
    for i in range(units + 3):
        if i < units:
            passed(order[i])
            if i == 0:
                each(nz, z, lambda d: tk_copy(d, z).wait_recv())
            first_matmul(order[i])
        if 0 <= i - 1 < units:
            rs_step(order[i - 1], 1)
        if 0 <= i - 2 < units:
            rs_step(order[i - 2], 3)
        if i < units - 1:
            arrivals(order[i + 1])
        if i < units:
            chip_sum(order[i])
        if 0 <= i - 1 < units:
            rs_step(order[i - 1], 2)
        if 0 <= i - 2 < units:
            activate(order[i - 2])
        if 0 <= i - 3 < units:
            pass_on(order[i - 3])
        if i == units:
            for j in range(eh // 2):
                each(nz, z, lambda d: w2_copy(j, d, z).wait_recv())
                f2_copy(j, y).start()
            for store in stores[:2]:
                store.start()
            osg[...] = osh[0].reshape(ff, width)
            osu[...] = osh[1].reshape(ff, width)
            osd[...] = osh[2].reshape(ff, width)
            for store in stores[3:]:
                store.start()
        if i == units + 1:
            for j in range(eh // 2):
                f2_copy(j, 1 - y).wait_recv()
            for u in range(eh):
                all_hidden(u)
                res = nn_dot(hidden_part(u, 0), o2[u, :half, :]) + nn_dot(hidden_part(u, 1), o2[u, half:, :])
                rb[:, CAPACITY * u : CAPACITY * (u + 1), :] = res.reshape(nz, CAPACITY, width).astype(BF16)
                each(nz, z, lambda d: re_copy(u, z, d).start())
            stores[2].start()
    rt[z] = rb[z]
    all_hidden(eh)
    down = osh[2].reshape(ff, width)
    shared = nn_dot(hidden_part(eh, 0), down[:half]) + nn_dot(hidden_part(eh, 1), down[half:])
    for u in range(eh):
        each(nz, z, lambda d: re_copy(u, d, z).wait_recv())
    back = rt[...].reshape(experts * CAPACITY, width)
    out_ref[...] = (nn_dot(sel_hi[...], back) + nn_dot(sel_lo[...], back) + shared).astype(BF16)

    for store in stores:
        store.wait()
    each(nt, t, lambda d: stat_copy(t, d).wait_send())
    each(nz, z, lambda d: tk_copy(z, d).wait_send())

    def sent(side):
        for e in range(eh):
            each(nz, z, lambda d: w1_copy(side, e, z, d).wait_send())
            f1_copy(e, side).wait_send()

    on_side(sent)
    for j in range(eh // 2):
        each(nz, z, lambda d: w2_copy(j, z, d).wait_send())
        f2_copy(j, y).wait_send()
    each(nz, z, lambda d: sh_copy(z, d).wait_send())
    fs_copy(y).wait_send()
    for u in range(units):
        dd_copy(u).wait_send()
        for k in range(n_long):
            rs_copy(u, 0, k).wait_send()
        for k in range(n_short):
            rs_copy(u, 1, k).wait_send()
        each(nx, x, lambda d: ag_copy(u, x, d).wait_send())
        fw_copy(u, x, core).wait_send()
        each(nx, x, lambda d: fw_copy(u, d, core).wait_send())
    for u in range(eh):
        each(nz, z, lambda d: re_copy(u, z, d).wait_send())


def hand_over(*refs):
    n = len(refs) // 3
    took, gave = refs[3 * n], refs[3 * n + 1]
    ins = [pltpu.make_async_copy(refs[i], refs[2 * n + i], took.at[i]) for i in range(n)]
    outs = [pltpu.make_async_copy(refs[2 * n + i], refs[n + i], gave.at[i]) for i in range(n)]
    for copy in ins:
        copy.start()
    for i in range(n):
        ins[i].wait()
        outs[i].start()
    for copy in outs:
        copy.wait()


def on_device(nz, nt, tokens, norm_gain, expert_ids, route_scores, gate, up, down, sg, su, sd):
    experts, ff_here, width = gate.shape
    eh = experts // nz
    ff = ff_here * nz
    half = ff // 2
    toks = tokens.shape[0]
    nx = nt // 2
    rows = eh * nz * CAPACITY + toks
    disp = (nz, eh * CAPACITY, width)
    units = eh + 1
    vmem = pl.BlockSpec(memory_space=pltpu.VMEM)
    dma = pltpu.SemaphoreType.DMA
    pairs = eh // 2
    sems = []
    for shape in (
        (nt,), (nz,), (eh, nz), (eh,), (pairs, nz), (pairs,), (nz,), (), (units,), (units, nx - 1), (units, nx),
        (units, nx), (eh, nz),
    ):
        sems += [dma(shape), dma(shape)]
    anyw = pl.BlockSpec(memory_space=pl.ANY)
    made = pl.pallas_call(
        functools.partial(layer_kernel, nz, nt, width * nt),
        out_shape=(
            *([jax.ShapeDtypeStruct((eh, ff, width), BF16)] * 3),
            *([jax.ShapeDtypeStruct((ff, width), BF16)] * 3),
            jax.ShapeDtypeStruct((toks, width), BF16),
        ),
        in_specs=[vmem] * 4 + [anyw] * 3 + [vmem] * 3,
        out_specs=(anyw,) * 6 + (vmem,),
        scratch_shapes=[
            *([pltpu.VMEM((experts, ff_here, width), F32)] * 3),
            *([pltpu.VMEM((eh, ff, width), BF16)] * 3),
            *([pltpu.VMEM((ff, width), BF16)] * 3),
            dma((3,)),
            dma((6,)),
            pltpu.VMEM((3, nz, 2, ff_here // 2, width), BF16),
            pltpu.VMEM((2, experts, ff_here, width), BF16),
            pltpu.VMEM((experts, ff_here, width), BF16),
            pltpu.VMEM((3, 2, ff_here // 2, width), BF16),
            pltpu.VMEM((nt, 8, toks), F32),
            pltpu.VMEM(disp, BF16),
            pltpu.VMEM(disp, BF16),
            pltpu.VMEM((rows, 2 * half), F32),
            pltpu.VMEM((rows, 2 * half), BF16),
            pltpu.VMEM((rows, 2 * half), BF16),
            pltpu.VMEM((nx, rows // nx, 2 * half), BF16),
            pltpu.VMEM((nx - 1, rows // nx, 2 * half), BF16),
            pltpu.VMEM((2, nx, rows // nx, half), BF16),
            pltpu.VMEM(disp, BF16),
            pltpu.VMEM(disp, BF16),
            pltpu.VMEM((toks, experts * CAPACITY), BF16),
            pltpu.VMEM((toks, experts * CAPACITY), BF16),
            pltpu.VMEM((toks, width), BF16),
            *sems,
        ],
        compiler_params=pltpu.CompilerParams(
            collective_id=0, has_side_effects=True, vmem_limit_bytes=56 * 1024 * 1024
        ),
        name="layer",
    )(
        tokens, norm_gain.reshape(1, width), expert_ids.T, route_scores.T,
        gate, up, down, sg, su, sd,
    )
    return pl.pallas_call(
        hand_over,
        out_shape=tuple(jax.ShapeDtypeStruct(a.shape, a.dtype) for a in made),
        in_specs=[anyw] * len(made),
        out_specs=(anyw,) * len(made),
        scratch_shapes=[
            *(pltpu.VMEM(a.shape, a.dtype) for a in made),
            dma((len(made),)),
            dma((len(made),)),
        ],
        name="hand_over",
    )(*made)


def solution(mesh):
    return jax.shard_map(
        functools.partial(on_device, mesh.shape["fs"], mesh.shape["tp"]),
        mesh=mesh,
        in_specs=(
            P(("grp", "fs"), "tp"),
            P("tp"),
            P(("grp", "fs"), None),
            P(("grp", "fs"), None),
            P(None, "fs", "tp"),
            P(None, "fs", "tp"),
            P(None, "fs", "tp"),
            P("fs", "tp"),
            P("fs", "tp"),
            P("fs", "tp"),
        ),
        out_specs=(
            P(("grp", "fs"), None, "tp"),
            P(("grp", "fs"), None, "tp"),
            P(("grp", "fs"), None, "tp"),
            P("grp", "tp"),
            P("grp", "tp"),
            P("grp", "tp"),
            P(("grp", "fs"), "tp"),
        ),
        check_vma=False,
    )
```

time: 182 us -> 164 us (0.901)
  Pallas kernels: 174 us -> 163 us
  local copies, waits for them, and re-layouts: 7.04 us -> 0 us
    pallas_call x1, Pallas kernels: 174 us -> 160 us  [on_device(): pl.pallas_call(functools.partial(layer_kernel, nz, nt, width * nt), out_s...]
    unnamed x12 -> x0, local copies, waits for them, and re-layouts: 4 us -> none
    pallas_call x0 -> x1, Pallas kernels: none -> 2.43 us  [on_device(): pl.pallas_call(hand_over, out_shape=tuple((jax.ShapeDtypeStruct(a.shape,...]
    squeeze x1 -> x0, local copies, waits for them, and re-layouts: 2.29 us -> none  [on_device(): return (o1[0], o1[1], o2, osh[0], osh[1], osh[2], out)]
where the time goes in v2:
time: 164 us; the launch traced here: 163 us
  Pallas kernels  163 us (99%)
    pallas_call x1, Pallas kernels, on_device(): pl.pallas_call(functools.partial(layer_kernel, nz, nt, width * nt), out_s...  160 us

profile of v2, /device:TPU:65, one launch (start us, length us, event | category | flops | bytes accessed | tf_op | source)
XLA Modules:
  0.0 163.3 jit_solution(17209910266766692526)
XLA Ops:
  0.6 160.2 %layer.1 = (bf16[4,512,128]{2,1,0:T(8,128)(2,1)}, bf16[4,512,128]{2,1,0:T(8,128)(2,1)}, bf16[4,512,128]{2,1,0:T(8,128)(2,1)}, bf16[512,128]{1,0:T(8,128)(2,1)}, ...) custom-call(bf16[128,128]{1,0:T(8,128)(2,1)} %tok_ref.1, f32[1,128]{1,0:T(1,128)} %bitcast.5, ...), custom_call_target="tpu_custom_call" | custom-call | tf_op jit(solution)/shard_map/layer/pallas_call | solution.py:443
  160.8 2.4 %hand_over.1 = (bf16[4,512,128]{2,1,0:T(8,128)(2,1)}, bf16[4,512,128]{2,1,0:T(8,128)(2,1)}, bf16[4,512,128]{2,1,0:T(8,128)(2,1)}, bf16[512,128]{1,0:T(8,128)(2,1...) custom-call(bf16[4,512,128]{2,1,0:T(8,128)(2,1)} %get-tuple-element.14.refs_0_, ...), custom_call_target="tpu_custom_call" | custom-call | tf_op jit(solution)/shard_map/hand_over/pallas_call | solution.py:486

commit v3 on v2

--- a/solution.py
+++ b/solution.py
@@ -28,7 +28,7 @@
     tok_ref, gain_ref, ids_ref, score_ref, gate_hbm, up_hbm, down_hbm, sg_ref, su_ref, sd_ref,
     og_hbm, ou_hbm, od_hbm, osg_hbm, osu_hbm, osd_hbm, out_ref,
     gate_ref, up_ref, down_ref, og, ou, o2, osg, osu, osd, in_sem, out_sem,
-    osh, w1, w2, ws, stat, xs, xr, own, pdo, pdr, q, rr, h, rb, rt, sel_hi, sel_lo, nrm_ref,
+    osh, w1, w2, ws, stat, xs, xr, own, pdo, pdr, q, rr, h, rb, rt, sel, nrm_ref,
     st_s, st_r, tk_s, tk_r, w1_s, w1_r, f1_s, f1_r, w2_s, w2_r, f2_s, f2_r, sh_s, sh_r, fs_s, fs_r,
     dd_s, dd_r, rs_s, rs_r, ag_s, ag_r, fw_s, fw_r, re_s, re_r,
 ):
@@ -146,8 +146,9 @@
     def sh_copy(src, dst):
         return rcopy(ws.at[:, y], osh.at[:, src, y], sh_s.at[dst], sh_r.at[src], fs=dst)
 
-    def tk_copy(src, dst):
-        return rcopy(xs.at[dst], xr.at[src], tk_s.at[dst], tk_r.at[src], fs=dst)
+    def tk_copy(u, src, dst):
+        rows = pl.ds(CAPACITY * u, CAPACITY)
+        return rcopy(xs.at[dst, rows], xr.at[src, rows], tk_s.at[u, dst], tk_r.at[u, src], fs=dst)
 
     def send_w1(first, last):
         def one(side):
@@ -184,11 +185,13 @@
     nrm = ((tok_t - mean) * lax.rsqrt(var + NORM_EPS)).T.astype(BF16)
     nrm_ref[...] = nrm
     xs[...] = nn_dot(pick, nrm).astype(BF16).reshape(nz, eh * CAPACITY, width)
-    each(nz, z, lambda d: tk_copy(z, d).start())
-    send_w1(1, eh)
-    each(nz, z, lambda d: sh_copy(z, d).start())
+    for u in range(eh):
+        each(nz, z, lambda d: tk_copy(u, z, d).start())
+        if u + 1 < eh:
+            send_w1(u + 1, u + 2)
     for j in range(eh // 2):
         each(nz, z, lambda d: w2_copy(j, z, d).start())
+    each(nz, z, lambda d: sh_copy(z, d).start())
 
     xr[z] = xs[z]
     rank = jnp.concatenate([rank_t, jnp.full((toks - experts, toks), -1.0, F32)], axis=0).T
@@ -201,8 +204,8 @@
     mine = nn_dot(rank.astype(BF16), wide) == col_slot
     hi = spread.astype(BF16)
     lo = (spread - hi.astype(F32)).astype(BF16)
-    sel_hi[...] = jnp.where(mine, nn_dot(hi, wide), 0.0).astype(BF16)
-    sel_lo[...] = jnp.where(mine, nn_dot(lo, wide), 0.0).astype(BF16)
+    sel[:toks, :] = jnp.where(mine, nn_dot(hi, wide), 0.0).astype(BF16)
+    sel[toks:, :] = jnp.where(mine, nn_dot(lo, wide), 0.0).astype(BF16)
 
     def f1_copy(e, side):
         return rcopy(o1[side].at[e], o1[side].at[e], f1_s.at[e], f1_r.at[e], grp=mate)
@@ -221,6 +224,13 @@
 
     def turn(k):
         return lax.rem(x + k * ahead + nx, nx)
+
+    def across(k):
+        rows = pl.ds(*unit_rows(eh))
+        goal = lax.rem(x + k, nx)
+        return rcopy(
+            q.at[goal, rows], rr.at[k - 1, rows], rs_s.at[eh, k - 1], rs_r.at[eh, k - 1], tp=2 * goal + core
+        )
 
     def rs_copy(u, arm, k):
         r0, n = unit_rows(u)
@@ -254,7 +264,7 @@
     def first_matmul(u):
         r0, n = unit_rows(u)
         if u < eh:
-            arrived = xr[...].astype(F32)[:, u * CAPACITY : (u + 1) * CAPACITY, :]
+            arrived = xr[:, u * CAPACITY : (u + 1) * CAPACITY, :].astype(F32)
             rows_in = arrived.reshape(cap_rows, width).astype(BF16)
         else:
             rows_in = nrm_ref[...]
@@ -268,8 +278,12 @@
         dd_copy(u).wait_recv()
         both = own[rows, :] + pdr[rows, :].astype(F32)
         q[:, r0 : r0 + n, :] = both.astype(BF16).reshape(nx, n, 2 * half)
-        rs_copy(u, 0, 0).start()
-        rs_copy(u, 1, 0).start()
+        if u == eh:
+            for k in range(1, nx):
+                across(k).start()
+        else:
+            rs_copy(u, 0, 0).start()
+            rs_copy(u, 1, 0).start()
 
     def rs_step(u, k):
         r0, n = unit_rows(u)
@@ -284,9 +298,15 @@
     def activate(u):
         r0, n = unit_rows(u)
         rows = slice(r0, r0 + n)
-        rs_copy(u, 0, n_long - 1).wait_recv()
-        rs_copy(u, 1, n_short - 1).wait_recv()
-        pre = q[x, rows, :].astype(F32) + rr[n_long - 1, rows, :].astype(F32) + rr[nx - 2, rows, :].astype(F32)
+        pre = q[x, rows, :].astype(F32)
+        if u == eh:
+            for k in range(1, nx):
+                across(k).wait_recv()
+            pre = pre + jnp.sum(rr[:, rows, :].astype(F32), axis=0)
+        else:
+            rs_copy(u, 0, n_long - 1).wait_recv()
+            rs_copy(u, 1, n_short - 1).wait_recv()
+            pre = pre + rr[n_long - 1, rows, :].astype(F32) + rr[nx - 2, rows, :].astype(F32)
         h[core, x, r0 : r0 + n, :] = (jax.nn.silu(pre[:, :half]) * pre[:, half:]).astype(BF16)
         each(nx, x, lambda d: ag_copy(u, x, d).start())
         fw_copy(u, x, core).start()
@@ -326,61 +346,65 @@
         else:
             fs_copy(1 - y).wait_recv()
 
-    order = tuple(range(units))
-    arrivals(order[0])
-    for i in range(units + 3):
-        if i < units:
-            passed(order[i])
-            if i == 0:
-                each(nz, z, lambda d: tk_copy(d, z).wait_recv())
-            first_matmul(order[i])
-        if 0 <= i - 1 < units:
-            rs_step(order[i - 1], 1)
-        if 0 <= i - 2 < units:
-            rs_step(order[i - 2], 3)
-        if i < units - 1:
-            arrivals(order[i + 1])
-        if i < units:
-            chip_sum(order[i])
-        if 0 <= i - 1 < units:
-            rs_step(order[i - 1], 2)
-        if 0 <= i - 2 < units:
-            activate(order[i - 2])
-        if 0 <= i - 3 < units:
-            pass_on(order[i - 3])
-        if i == units:
+    def second_matmul(u):
+        all_hidden(u)
+        res = nn_dot(hidden_part(u, 0), o2[u, :half, :]) + nn_dot(hidden_part(u, 1), o2[u, half:, :])
+        rb[:, CAPACITY * u : CAPACITY * (u + 1), :] = res.reshape(nz, CAPACITY, width).astype(BF16)
+        each(nz, z, lambda d: re_copy(u, z, d).start())
+
+    arrivals(0)
+    for i in range(eh + 2):
+        if i < eh:
+            passed(i)
+            each(nz, z, lambda d: tk_copy(i, d, z).wait_recv())
+            first_matmul(i)
+        if 0 <= i - 1 < eh:
+            rs_step(i - 1, 1)
+        if 0 <= i - 2 < eh:
+            rs_step(i - 2, 3)
+        if i < eh - 1:
+            arrivals(i + 1)
+        if i < eh:
+            chip_sum(i)
+        if 0 <= i - 1 < eh:
+            rs_step(i - 1, 2)
+        if 0 <= i - 2 < eh:
+            activate(i - 2)
+        if 0 <= i - 3 < eh:
+            pass_on(i - 3)
+        if i == eh:
             for j in range(eh // 2):
                 each(nz, z, lambda d: w2_copy(j, d, z).wait_recv())
                 f2_copy(j, y).start()
             for store in stores[:2]:
                 store.start()
-            osg[...] = osh[0].reshape(ff, width)
-            osu[...] = osh[1].reshape(ff, width)
-            osd[...] = osh[2].reshape(ff, width)
-            for store in stores[3:]:
-                store.start()
-        if i == units + 1:
-            for j in range(eh // 2):
-                f2_copy(j, 1 - y).wait_recv()
-            for u in range(eh):
-                all_hidden(u)
-                res = nn_dot(hidden_part(u, 0), o2[u, :half, :]) + nn_dot(hidden_part(u, 1), o2[u, half:, :])
-                rb[:, CAPACITY * u : CAPACITY * (u + 1), :] = res.reshape(nz, CAPACITY, width).astype(BF16)
-                each(nz, z, lambda d: re_copy(u, z, d).start())
-            stores[2].start()
+    for j in range(eh // 2):
+        f2_copy(j, 1 - y).wait_recv()
+    for u in range(eh - 1):
+        second_matmul(u)
+    arrivals(eh)
+    pass_on(eh - 1)
+    second_matmul(eh - 1)
+    passed(eh)
+    first_matmul(eh)
+    chip_sum(eh)
+    stores[2].start()
+    osg[...] = osh[0].reshape(ff, width)
+    osu[...] = osh[1].reshape(ff, width)
+    osd[...] = osh[2].reshape(ff, width)
+    for store in stores[3:]:
+        store.start()
+    activate(eh)
+    pass_on(eh)
     rt[z] = rb[z]
     all_hidden(eh)
     down = osh[2].reshape(ff, width)
     shared = nn_dot(hidden_part(eh, 0), down[:half]) + nn_dot(hidden_part(eh, 1), down[half:])
-    for u in range(eh):
-        each(nz, z, lambda d: re_copy(u, d, z).wait_recv())
-    back = rt[...].reshape(experts * CAPACITY, width)
-    out_ref[...] = (nn_dot(sel_hi[...], back) + nn_dot(sel_lo[...], back) + shared).astype(BF16)
-
     for store in stores:
         store.wait()
     each(nt, t, lambda d: stat_copy(t, d).wait_send())
-    each(nz, z, lambda d: tk_copy(z, d).wait_send())
+    for u in range(eh):
+        each(nz, z, lambda d: tk_copy(u, z, d).wait_send())
 
     def sent(side):
         for e in range(eh):
@@ -395,15 +419,24 @@
     fs_copy(y).wait_send()
     for u in range(units):
         dd_copy(u).wait_send()
-        for k in range(n_long):
-            rs_copy(u, 0, k).wait_send()
-        for k in range(n_short):
-            rs_copy(u, 1, k).wait_send()
+        if u == eh:
+            for k in range(1, nx):
+                across(k).wait_send()
+        else:
+            for k in range(n_long):
+                rs_copy(u, 0, k).wait_send()
+            for k in range(n_short):
+                rs_copy(u, 1, k).wait_send()
         each(nx, x, lambda d: ag_copy(u, x, d).wait_send())
         fw_copy(u, x, core).wait_send()
         each(nx, x, lambda d: fw_copy(u, d, core).wait_send())
     for u in range(eh):
         each(nz, z, lambda d: re_copy(u, z, d).wait_send())
+    for u in range(eh):
+        each(nz, z, lambda d: re_copy(u, d, z).wait_recv())
+    back = rt[...].reshape(experts * CAPACITY, width)
+    mixed = nn_dot(sel[...], back)
+    out_ref[...] = (mixed[:toks] + mixed[toks:] + shared).astype(BF16)
 
 
 def hand_over(*refs):
@@ -435,7 +468,7 @@
     pairs = eh // 2
     sems = []
     for shape in (
-        (nt,), (nz,), (eh, nz), (eh,), (pairs, nz), (pairs,), (nz,), (), (units,), (units, nx - 1), (units, nx),
+        (nt,), (eh, nz), (eh, nz), (eh,), (pairs, nz), (pairs,), (nz,), (), (units,), (units, nx - 1), (units, nx),
         (units, nx), (eh, nz),
     ):
         sems += [dma(shape), dma(shape)]
@@ -470,8 +503,7 @@
             pltpu.VMEM((2, nx, rows // nx, half), BF16),
             pltpu.VMEM(disp, BF16),
             pltpu.VMEM(disp, BF16),
-            pltpu.VMEM((toks, experts * CAPACITY), BF16),
-            pltpu.VMEM((toks, experts * CAPACITY), BF16),
+            pltpu.VMEM((2 * toks, experts * CAPACITY), BF16),
             pltpu.VMEM((toks, width), BF16),
             *sems,
         ],

time: 164 us -> 155 us (0.945)
  Pallas kernels: 163 us -> 154 us
    pallas_call x1, Pallas kernels: 160 us -> 152 us  [on_device(): pl.pallas_call(functools.partial(layer_kernel, nz, nt, width * nt), out_s...]
where the time goes in v3:
time: 155 us
  Pallas kernels  154 us (99%)
    pallas_call x1, Pallas kernels, on_device(): pl.pallas_call(functools.partial(layer_kernel, nz, nt, width * nt), out_s...  152 us

profile of v3, /device:TPU:65, one launch (start us, length us, event | category | flops | bytes accessed | tf_op | source)
XLA Modules:
  0.0 155.1 jit_solution(6136598675426502274)
XLA Ops:
  0.6 152.0 %layer.1 = (bf16[4,512,128]{2,1,0:T(8,128)(2,1)}, bf16[4,512,128]{2,1,0:T(8,128)(2,1)}, bf16[4,512,128]{2,1,0:T(8,128)(2,1)}, bf16[512,128]{1,0:T(8,128)(2,1)}, ...) custom-call(bf16[128,128]{1,0:T(8,128)(2,1)} %tok_ref.1, f32[1,128]{1,0:T(1,128)} %bitcast.5, ...), custom_call_target="tpu_custom_call" | custom-call | tf_op jit(solution)/shard_map/layer/pallas_call | solution.py:476
  152.7 2.4 %hand_over.1 = (bf16[4,512,128]{2,1,0:T(8,128)(2,1)}, bf16[4,512,128]{2,1,0:T(8,128)(2,1)}, bf16[4,512,128]{2,1,0:T(8,128)(2,1)}, bf16[512,128]{1,0:T(8,128)(2,1...) custom-call(bf16[4,512,128]{2,1,0:T(8,128)(2,1)} %get-tuple-element.14.refs_0_, ...), custom_call_target="tpu_custom_call" | custom-call | tf_op jit(solution)/shard_map/hand_over/pallas_call | solution.py:518
